TPU v7x, 32 devices: a whole 2x2x4 slice. The times are simulated.
32 devices in a mesh: ep: 8 (over z, y), tp: 4 (over x, core).
Axes of the slice: x: 2, y: 2, z: 4, core: 2. Of those that a mesh axis runs over, the one named last changes fastest.
Arguments:
- tokens: bfloat16 [2048, 1024], P('ep'), may hold values from -6 to 6
- cotangent: bfloat16 [2048, 1024], P('ep'), may hold values from -1.5 to 1.5
- routing: int32 [2048, 2], P('ep'), may hold values from 0 to 15, all different within a row; in each aligned block of 256 rows (0 to 255, 256 to 511, ...) at most 96 rows name the same one
- gate_weights: float32 [2048, 2], P('ep'), may hold values from 0.1 to 0.9
- gate_proj: bfloat16 [16, 1024, 512], P('ep', None, 'tp'), may hold values from -0.1875 to 0.1875
- up_proj: bfloat16 [16, 1024, 512], P('ep', None, 'tp'), may hold values from -0.1875 to 0.1875
- down_proj: bfloat16 [16, 512, 1024], P('ep', 'tp'), may hold values from -0.25 to 0.25
Outputs:
- tokens_grad: bfloat16 [2048, 1024], P('ep')
- gates_grad: float32 [2048, 2], P('ep')
- gate_proj_grad: float32 [16, 1024, 512], P('ep', None, 'tp')
- up_proj_grad: float32 [16, 1024, 512], P('ep', None, 'tp')
- down_proj_grad: float32 [16, 512, 1024], P('ep', 'tp')
Inputs may be any that keep to these rules, and one draw needn't show every extreme that they name: `routing`: each row names 2 different experts; every expert is named by some row; within each aligned block of 256 rows (the tokens of one index of ep) no expert is named by more than 96 rows, a bound that some block reaches.
All inputs are finite; a program needn't handle non-finite values.
Results may differ from a plain program's by a relative error of at most 0.0015.
Values may be sent and summed in bfloat16 or wider, within the bound.
A program may use at most 128 MiB of HBM per device.

v0:
```python
import jax
import jax.numpy as jnp
from jax import lax
from jax.sharding import PartitionSpec as P


def expert_terms(expert_rows, expert_scaled, gate_proj, up_proj, down_proj):
    gate_pre = jnp.einsum(
        "erd,edf->erf", expert_rows, gate_proj, preferred_element_type=jnp.float32
    ).astype(jnp.bfloat16)
    up_pre = jnp.einsum(
        "erd,edf->erf", expert_rows, up_proj, preferred_element_type=jnp.float32
    ).astype(jnp.bfloat16)
    gate_pre, up_pre = lax.optimization_barrier((gate_pre, up_pre))
    hidden_grad = jnp.einsum(
        "erd,efd->erf", expert_scaled, down_proj, preferred_element_type=jnp.float32
    )
    gate_wide = gate_pre.astype(jnp.float32)
    up_wide = up_pre.astype(jnp.float32)
    sigmoid_gate = jax.nn.sigmoid(gate_wide)
    activated = gate_wide * sigmoid_gate
    hidden = activated * up_wide
    product = jnp.sum(hidden_grad * hidden, axis=-1)
    gate_pre_grad = (
        hidden_grad * up_wide * sigmoid_gate * (1.0 + gate_wide * (1.0 - sigmoid_gate))
    ).astype(jnp.bfloat16)
    up_pre_grad = (hidden_grad * activated).astype(jnp.bfloat16)
    input_grad = jnp.einsum(
        "erf,edf->erd", gate_pre_grad, gate_proj, preferred_element_type=jnp.float32
    )
    input_grad = input_grad + jnp.einsum(
        "erf,edf->erd", up_pre_grad, up_proj, preferred_element_type=jnp.float32
    )
    down_grad = jnp.einsum(
        "erf,erd->efd",
        hidden.astype(jnp.bfloat16),
        expert_scaled,
        preferred_element_type=jnp.float32,
    )
    gate_grad = jnp.einsum(
        "erd,erf->edf", expert_rows, gate_pre_grad, preferred_element_type=jnp.float32
    )
    up_grad = jnp.einsum(
        "erd,erf->edf", expert_rows, up_pre_grad, preferred_element_type=jnp.float32
    )
    return (input_grad, product, gate_grad, up_grad, down_grad)


def shards(tokens, cotangent, routing, gate_weights, gate_proj, up_proj, down_proj):
    token_count, model_width = tokens.shape
    top_count = routing.shape[1]
    local_experts = gate_proj.shape[0]
    groups = lax.axis_size("ep")
    members = lax.axis_size("tp")
    experts = local_experts * groups
    capacity = members * (
        (3 * token_count * top_count + experts * members - 1) // (experts * members)
    )
    slot_count = experts * capacity
    pair_count = token_count * top_count
    pair_expert = routing.reshape(pair_count)
    onehot = (pair_expert[:, None] == jnp.arange(experts, dtype=jnp.int32)[None, :]).astype(
        jnp.int32
    )
    position = jnp.sum(jnp.cumsum(onehot, axis=0) * onehot, axis=1) - 1
    pair_slot = pair_expert * capacity + position
    pair_number = jnp.arange(pair_count, dtype=jnp.int32)
    owner_pair = jnp.zeros((slot_count,), jnp.int32).at[pair_slot].set(pair_number)
    filled = jnp.zeros((slot_count,), jnp.int32).at[pair_slot].set(1) > 0
    owner_token = owner_pair // top_count
    slot_weight = jnp.where(filled, gate_weights.reshape(pair_count)[owner_pair], 0.0)
    send_rows = jnp.where(filled[:, None], tokens[owner_token], jnp.zeros((), jnp.bfloat16))
    send_scaled = (slot_weight[:, None] * cotangent[owner_token].astype(jnp.float32)).astype(
        jnp.bfloat16
    )
    layout = (groups, local_experts, capacity, model_width)
    send_rows = send_rows.reshape(layout)
    send_scaled = send_scaled.reshape(layout)
    quarter = capacity // members
    quarter_start = lax.axis_index("tp") * quarter
    part_rows = lax.dynamic_slice_in_dim(send_rows, quarter_start, quarter, 2)
    part_scaled = lax.dynamic_slice_in_dim(send_scaled, quarter_start, quarter, 2)
    landed = (
        lax.all_to_all(part_rows, "ep", split_axis=0, concat_axis=0, tiled=True),
        lax.all_to_all(part_scaled, "ep", split_axis=0, concat_axis=0, tiled=True),
    )
    recv_rows, recv_scaled = (
        lax.all_gather(landed[0], "tp", axis=2, tiled=True),
        lax.all_gather(landed[1], "tp", axis=2, tiled=True),
    )
    expert_rows = recv_rows.transpose(1, 0, 2, 3).reshape(
        local_experts, groups * capacity, model_width
    )
    expert_scaled = recv_scaled.transpose(1, 0, 2, 3).reshape(
        local_experts, groups * capacity, model_width
    )
    input_grad, product, gate_grad, up_grad, down_grad = expert_terms(
        expert_rows, expert_scaled, gate_proj, up_proj, down_proj
    )
    input_grad = input_grad.reshape(local_experts, groups, capacity, model_width).transpose(
        1, 0, 2, 3
    )
    product = product.reshape(local_experts, groups, capacity).transpose(1, 0, 2)
    back_grad, back_product = (
        lax.all_to_all(input_grad, "ep", split_axis=0, concat_axis=0, tiled=True),
        lax.all_to_all(product, "ep", split_axis=0, concat_axis=0, tiled=True),
    )
    local_slot = position
    present = (local_slot >= 0) & (local_slot < capacity)
    back_index = pair_expert * capacity + jnp.clip(local_slot, 0, capacity - 1)
    pair_grad = jnp.where(
        present[:, None], back_grad.reshape(experts * capacity, model_width)[back_index], 0.0
    )
    pair_product = jnp.where(present, back_product.reshape(experts * capacity)[back_index], 0.0)
    token_grad = jnp.sum(pair_grad.reshape(token_count, top_count, model_width), axis=1)
    total_grad, total_product = lax.psum((token_grad, pair_product), "tp")
    tokens_grad = total_grad.astype(jnp.bfloat16)
    gates_grad = (total_product / gate_weights.reshape(pair_count)).reshape(token_count, top_count)
    return (tokens_grad, gates_grad, gate_grad, up_grad, down_grad)


def solution(mesh):
    in_specs = (
        P("ep", None),
        P("ep", None),
        P("ep", None),
        P("ep", None),
        P("ep", None, "tp"),
        P("ep", None, "tp"),
        P("ep", "tp", None),
    )
    out_specs = (
        P("ep", None),
        P("ep", None),
        P("ep", None, "tp"),
        P("ep", None, "tp"),
        P("ep", "tp", None),
    )
    return jax.shard_map(shards, mesh=mesh, in_specs=in_specs, out_specs=out_specs, check_vma=False)
```

profile of v0, /device:TPU:0, one launch (start us, length us, event | category | flops | bytes accessed | tf_op | source)
XLA Modules:
  0.0 327.0 jit_solution(3575784898565409781)
XLA Ops:
  7.2 0.7 broadcast_multiply_fusion
  8.0 0.8 copy.62
  8.8 0.1 eq.29
  8.9 0.1 eq.25
  9.1 0.1 copy.65
  9.2 0.1 mul.61
  9.4 1.2 reduce-window.6
  10.5 0.2 slice_reduce_fusion
  10.8 0.1 fusion.12
  10.9 2.5 scatter_custom_fusion.1
  13.4 2.5 scatter_custom_fusion
  15.9 0.8 copy.66
  16.7 0.1 reshape.148
  16.9 9.5 %gather_fusion = f32[1536]{0:T(1024)S(1)} fusion(f32[512]{0:T(512)S(1)} %reshape.148, s32[2048]{0:T(1024)S(1)} %get-tuple-element.38), kind=kCustom, calls=%fused_computation | custom fusion | bytes 18432 | tf_op jit(solution)/shard_map/gather | solution.py:71
  26.5 5.8 %gather_fusion.2 = bf16[1536,1024]{1,0:T(8,128)(2,1)} fusion(bf16[256,1024]{1,0:T(8,128)(2,1)S(1)} %copy-done.1, s32[2048]{0:T(1024)S(1)} %get-tuple-element.37), kind=kCustom, calls=%fused_computation.2 | custom fusion | bytes 6297600 | tf_op jit(solution)/shard_map/gather | solution.py:72
  32.3 1.4 dynamic-slice_select_fusion
  33.7 27.8 %all_to_all.20 = bf16[8,2,24,1024]{3,2,1,0:T(8,128)(2,1)} all-to-all(bf16[8,2,24,1024]{3,2,1,0:T(8,128)(2,1)S(1)} %dynamic-slice_select_fusion), channel_id=1, replica_groups=mesh['ep'=8,'tp'=4] {'ep'}, dimensions={0} | all-to-all | bytes 1572864 | tf_op jit(solution)/shard_map/all_to_all | solution.py:84
  61.7 5.8 %gather_fusion.1 = bf16[1536,1024]{1,0:T(8,128)(2,1)} fusion(bf16[256,1024]{1,0:T(8,128)(2,1)S(1)} %copy-done.2, s32[2048]{0:T(1024)S(1)} %get-tuple-element.37), kind=kCustom, calls=%fused_computation.1 | custom fusion | bytes 6297600 | tf_op jit(solution)/shard_map/gather | solution.py:73
  67.6 1.3 fusion
  68.9 23.5 %all_to_all.21 = bf16[8,2,24,1024]{3,2,1,0:T(8,128)(2,1)} all-to-all(bf16[8,2,24,1024]{3,2,1,0:T(8,128)(2,1)S(1)} %fusion), channel_id=1, replica_groups=mesh['ep'=8,'tp'=4] {'ep'}, dimensions={0} | all-to-all | bytes 1572864 | tf_op jit(solution)/shard_map/all_to_all | solution.py:85
  92.5 2.4 copy.68
  94.9 1.2 convolution_convert_fusion
  96.1 0.4 copy-done.3
  96.6 1.2 convolution_convert_fusion.1
  97.7 23.6 %all-gather.3.cloned.1.call-done = bf16[8,2,96,1024]{3,2,1,0:T(8,128)(2,1)} async-done(((bf16[8,2,24,1024]{3,2,1,0:T(8,128)(2,1)}), bf16[8,2,96,1024]{3,2,1,0:T(8,128)(2,1)}) %all-gather.3.cloned.1.call-update) | async-done | bytes 3145744 | tf_op jit(solution)/shard_map/all_gather | solution.py:89
  121.3 2.4 copy.67
  123.7 1.4 multiply_reduce_fusion
  125.1 0.3 copy-done.5
  125.4 0.6 copy.74
  126.0 5.5 %all-to-all-start.3 = ((f32[8,2,96]{2,1,0:T(2,128)}), f32[8,2,96]{2,1,0:T(2,128)S(1)}, u32[]{:S(2)}, u32[]{:S(2)}) async-start(f32[8,2,96]{2,1,0:T(2,128)} %copy.74), calls=%async_computation.3 | async-start | bytes 16384 | tf_op jit(solution)/shard_map/all_to_all | solution.py:106
  131.5 1.0 fusion.21
  132.6 1.1 convolution_add_fusion
  133.7 3.2 copy.91
  136.9 1.2 all-to-all-done.3
  138.1 4.8 %all-to-all-start.2 = ((f32[8,2,96,1024]{3,2,1,0:T(8,128)}), f32[8,2,96,1024]{3,2,1,0:T(8,128)}, u32[]{:S(2)}, u32[]{:S(2)}) async-start(f32[8,2,96,1024]{3,2,1,0:T(8,128)} %bitcast.50), calls=%async_computation.2 | async-start | bytes 12582912 | tf_op jit(solution)/shard_map/all_to_all | solution.py:105
  142.9 4.4 %fusion.22 = f32[2,1024,128]{2,1,0:T(8,128)} fusion(bf16[2,768,1024]{2,1,0:T(8,128)(2,1)} %bitcast.48, bf16[2,768,128]{1,2,0:T(8,128)(2,1)S(1)} %get-tuple-element.31), kind=kOutput, calls=%fused_computation.67 | convolution fusion | flops 402653184 | bytes 4587520 | tf_op jit(solution)/shard_map/erd,erf->edf/dot_general | solution.py:40
  147.3 1.8 fusion.9
  149.0 0.5 copy-done.4
  149.5 2.4 fusion.20
  152.0 3.1 gather_fusion.4
  155.1 0.2 and.17
  155.3 125.9 %all-to-all-done.2 = f32[8,2,96,1024]{3,2,1,0:T(8,128)} async-done(((f32[8,2,96,1024]{3,2,1,0:T(8,128)}), f32[8,2,96,1024]{3,2,1,0:T(8,128)}, u32[]{:S(2)}, u32[]{:S(2)}) %all-to-all-start.2) | async-done | bytes 6291488 | tf_op jit(solution)/shard_map/all_to_all | solution.py:105
  281.2 5.6 %gather_fusion.3 = f32[512,1024]{1,0:T(8,128)S(1)} fusion(f32[1536,1024]{1,0:T(8,128)} %bitcast.11, s32[1024]{0:T(1024)S(1)} %pad_clamp_fusion.2), kind=kCustom, calls=%fused_computation.3 | custom fusion | bytes 4196352 | tf_op jit(solution)/shard_map/gather | solution.py:112
  286.8 2.3 gather.24
  289.1 4.1 %select_reduce_fusion = f32[256,1024]{1,0:T(8,128)S(1)} fusion(f32[256,2,1024]{2,1,0:T(2,128)} %gather.24, pred[256,2]{1,0:T(8,128)(4,1)S(1)} %and.17), kind=kLoop, calls=%fused_computation.9 | loop fusion | flops 786432 | bytes 3146240 | tf_op jit(solution)/shard_map/reduce_sum | solution.py:115
  293.3 26.0 %all-reduce.2 = (bf16[256,1024]{1,0:T(8,128)(2,1)}, f32[512]{0:T(512)S(1)}) all-reduce(f32[256,1024]{1,0:T(8,128)S(1)} %select_reduce_fusion, f32[512]{0:T(512)S(1)} %get-tuple-element.26), channel_id=1, replica_groups=mesh['ep'=8,'tp'=4] {'tp'}, use_global_device_ids=true, to_apply=%region_6.7 | all-reduce | flops 262656 | bytes 1576960 | tf_op jit(solution)/shard_map/psum | solution.py:116
  319.3 0.1 reshape.155
  319.5 0.7 copy.79
  (39 shorter events, 0.8 us)
Async XLA Ops:
  7.2 89.4 %copy-start = (bf16[2,1024,128]{2,1,0:T(8,128)(2,1)S(1)}, bf16[2,1024,128]{2,1,0:T(8,128)(2,1)}, u32[]{:S(2)}) copy-start(bf16[2,1024,128]{2,1,0:T(8,128)(2,1)} %param.11) | copy-start | bytes 1572868
  7.2 85.3 %all-gather.5.cloned.1.call-start = ((), (), s32[]{:S(2)}) async-start(), calls=%async_computation.5 | async-start | bytes 3932160 | tf_op jit(solution)/shard_map/all_gather | solution.py:88
  16.9 9.7 %copy-start.1 = (bf16[256,1024]{1,0:T(8,128)(2,1)S(1)}, bf16[256,1024]{1,0:T(8,128)(2,1)}, u32[]{:S(2)}) copy-start(bf16[256,1024]{1,0:T(8,128)(2,1)} %param.7) | copy-start | bytes 1572868
  32.3 29.4 %copy-start.2 = (bf16[256,1024]{1,0:T(8,128)(2,1)S(1)}, bf16[256,1024]{1,0:T(8,128)(2,1)}, u32[]{:S(2)}) copy-start(bf16[256,1024]{1,0:T(8,128)(2,1)} %param.8) | copy-start | bytes 1572868
  61.6 59.8 %all-gather.3.cloned.1.call-start = ((), (), s32[]{:S(2)}) async-start(), calls=%async_computation.4 | async-start | bytes 3932160 | tf_op jit(solution)/shard_map/all_gather | solution.py:89
  92.5 2.4 copy-start.7
  94.9 1.7 copy-start.3
  121.3 2.4 copy-start.8
  123.7 1.7 copy-start.5
  126.0 12.1 %all-to-all-start.3 = ((f32[8,2,96]{2,1,0:T(2,128)}), f32[8,2,96]{2,1,0:T(2,128)S(1)}, u32[]{:S(2)}, u32[]{:S(2)}) async-start(f32[8,2,96]{2,1,0:T(2,128)} %copy.74), calls=%async_computation.3 | async-start | bytes 16384 | tf_op jit(solution)/shard_map/all_to_all | solution.py:106
  138.1 143.1 %all-to-all-start.2 = ((f32[8,2,96,1024]{3,2,1,0:T(8,128)}), f32[8,2,96,1024]{3,2,1,0:T(8,128)}, u32[]{:S(2)}, u32[]{:S(2)}) async-start(f32[8,2,96,1024]{3,2,1,0:T(8,128)} %bitcast.50), calls=%async_computation.2 | async-start | bytes 12582912 | tf_op jit(solution)/shard_map/all_to_all | solution.py:105
  142.9 4.4 %copy-start.6 = (bf16[2,8,96,1024]{3,2,1,0:T(8,128)(2,1)S(1)}, bf16[2,8,96,1024]{3,2,1,0:T(8,128)(2,1)}, u32[]{:S(2)}) copy-start(bf16[2,8,96,1024]{3,2,1,0:T(8,128)(2,1)} %copy-done.5) | copy-start | bytes 9437188
  147.3 2.2 copy-start.4
Sparse Core Ops, SparseCore 0:
  61.7 27.0 all-gather.4
  92.6 28.6 all-gather.2
where the time goes:
time: 328 us; the launch traced here: 327 us
  waiting for transfers between devices  151 us (46%)
  blocking collectives  77.4 us (24%)
  local copies, waits for them, and re-layouts  50.8 us (15%)
  between operations  14.4 us (4%)
  matrix products  14.3 us (4%)
  starting transfers between devices  10.4 us (3%)
  other arithmetic  8.92 us (3%)
    all_to_all x1, waiting for transfers between devices, shards(): lax.all_to_all(input_grad, 'ep', split_axis=0, concat_axis=0, tiled=True)  126 us
    all_to_all x1, blocking collectives, shards(): lax.all_to_all(part_rows, 'ep', split_axis=0, concat_axis=0, tiled=True)  27.8 us
    psum x1, blocking collectives, shards(): total_grad, total_product = lax.psum((token_grad, pair_product), 'tp')  26 us
    all_gather x1, waiting for transfers between devices, shards(): lax.all_gather(landed[1], 'tp', axis=2, tiled=True)  23.6 us
    all_to_all x1, blocking collectives, shards(): lax.all_to_all(part_scaled, 'ep', split_axis=0, concat_axis=0, tiled=True)  23.5 us
    gather x1, local copies, waits for them, and re-layouts, shards(): gate_weights.reshape(pair_count)[owner_pair]  9.48 us
    gather x2, local copies, waits for them, and re-layouts, shards(): back_grad.reshape(experts * capacity, model_width)[back_index]  7.9 us
  transfers between devices with their start and end apart: 4, of which 3 were waited for; matrix products, arithmetic and copies ran while one was open for 9% of the time, Pallas kernels for 0%

commit v1 on v0

--- a/solution.py
+++ b/solution.py
@@ -46,7 +46,7 @@
     return (input_grad, product, gate_grad, up_grad, down_grad)
 
 
-def shards(tokens, cotangent, routing, gate_weights, gate_proj, up_proj, down_proj):
+def slot_shards(tokens, cotangent, routing, gate_weights, gate_proj, up_proj, down_proj):
     token_count, model_width = tokens.shape
     top_count = routing.shape[1]
     local_experts = gate_proj.shape[0]
@@ -119,6 +119,57 @@
     return (tokens_grad, gates_grad, gate_grad, up_grad, down_grad)
 
 
+def dense_shards(tokens, cotangent, routing, gate_weights, gate_proj, up_proj, down_proj):
+    token_count, model_width = tokens.shape
+    local_experts = gate_proj.shape[0]
+    groups = lax.axis_size("ep")
+    members = lax.axis_size("tp")
+    experts = local_experts * groups
+    all_axes = ("ep", "tp")
+    quarter = token_count // members
+    quarter_start = lax.axis_index("tp") * quarter
+    both = jnp.concatenate(
+        [
+            lax.dynamic_slice_in_dim(tokens, quarter_start, quarter, 0),
+            lax.dynamic_slice_in_dim(cotangent, quarter_start, quarter, 0),
+        ],
+        axis=1,
+    )
+    all_both = lax.all_gather(both, all_axes, axis=0, tiled=True)
+    chosen = routing[:, :, None] == jnp.arange(experts, dtype=jnp.int32)[None, None, :]
+    weights = jnp.sum(jnp.where(chosen, gate_weights[:, :, None], 0.0), axis=1)
+    all_weights = lax.all_gather(weights, "ep", axis=0, tiled=True)
+    first_expert = lax.axis_index("ep") * local_experts
+    my_weights = lax.dynamic_slice_in_dim(all_weights, first_expert, local_experts, 1)
+    all_tokens = all_both[:, :model_width]
+    all_cotangent = all_both[:, model_width:].astype(jnp.float32)
+    rows = jnp.broadcast_to(all_tokens[None], (local_experts,) + all_tokens.shape)
+    scaled = (my_weights.T[:, :, None] * all_cotangent[None]).astype(jnp.bfloat16)
+    input_grad, product, gate_grad, up_grad, down_grad = expert_terms(
+        rows, scaled, gate_proj, up_proj, down_proj
+    )
+    partial = jnp.sum(input_grad, axis=0)
+    own = jnp.zeros((token_count * groups, experts), jnp.float32)
+    own = lax.dynamic_update_slice_in_dim(own, product.T, first_expert, 1)
+    part_grad = lax.psum_scatter(partial, all_axes, scatter_dimension=0, tiled=True)
+    part_product = lax.psum_scatter(own, all_axes, scatter_dimension=0, tiled=True)
+    tokens_grad = lax.all_gather(part_grad.astype(jnp.bfloat16), "tp", axis=0, tiled=True)
+    block_product = lax.all_gather(part_product, "tp", axis=0, tiled=True)
+    pair_product = jnp.sum(jnp.where(chosen, block_product[:, None, :], 0.0), axis=2)
+    gates_grad = pair_product / gate_weights
+    return (tokens_grad, gates_grad, gate_grad, up_grad, down_grad)
+
+
+def shards(tokens, cotangent, routing, gate_weights, gate_proj, up_proj, down_proj):
+    token_count = tokens.shape[0]
+    experts = gate_proj.shape[0] * lax.axis_size("ep")
+    members = lax.axis_size("tp")
+    fair = token_count * routing.shape[1] // experts
+    dense = token_count <= 8 * fair and token_count % members == 0
+    plan = dense_shards if dense else slot_shards
+    return plan(tokens, cotangent, routing, gate_weights, gate_proj, up_proj, down_proj)
+
+
 def solution(mesh):
     in_specs = (
         P("ep", None),

time: 328 us -> 417 us (1.27)
  waiting for transfers between devices: 151 us -> 291 us
  local copies, waits for them, and re-layouts: 50.8 us -> 10.7 us
  blocking collectives: 77.4 us -> 44.1 us
  matrix products: 14.3 us -> 45.9 us
  starting transfers between devices: 10.4 us -> 0.3 us
    reduce_scatter x0 -> x1, waiting for transfers between devices: none -> 140 us  [dense_shards(): lax.psum_scatter(partial, all_axes, scatter_dimension=0, tiled=True)]
    all_to_all x2 -> x0, waiting for transfers between devices: 127 us -> none  [the longest x1 126 us: shards(): lax.all_to_all(input_grad, 'ep', split_axis=0, concat_axis=0, tiled=True)]
    unnamed x2 -> x4, waiting for transfers between devices: 0.03 us -> 102 us
    all_to_all x2 -> x0, blocking collectives: 51.3 us -> none  [the longest x1 27.8 us: shards(): lax.all_to_all(part_rows, 'ep', split_axis=0, concat_axis=0, tiled=True)]
    all_gather x0 -> x3, blocking collectives: none -> 44.1 us  [the longest x1 32.4 us: dense_shards(): all_weights = lax.all_gather(weights, 'ep', axis=0, tiled=True)]
    gather x6 -> x0, local copies, waits for them, and re-layouts: 32.1 us -> none  [the longest x1 9.48 us: shards(): gate_weights.reshape(pair_count)[owner_pair]]
    psum x1 -> x0, blocking collectives: 26 us -> none  [shards(): total_grad, total_product = lax.psum((token_grad, pair_product), 'tp')]
    all_gather x2 -> x1, waiting for transfers between devices: 23.6 us -> 49.2 us  [dense_shards(): all_both = lax.all_gather(both, all_axes, axis=0, tiled=True)]
  transfers between devices with their start and end apart: 4 -> 3, of which waited for: 3 -> 3; matrix products, arithmetic and copies ran while one was open for 9% -> 9% of each run, Pallas kernels for 0% -> 0%
where the time goes in v1:
time: 417 us
  waiting for transfers between devices  291 us (70%)
  matrix products  45.9 us (11%)
  blocking collectives  44.1 us (11%)
  between operations  14 us (3%)
  local copies, waits for them, and re-layouts  10.7 us (3%)
  other arithmetic  10.5 us (3%)
    reduce_scatter x1, waiting for transfers between devices, dense_shards(): lax.psum_scatter(partial, all_axes, scatter_dimension=0, tiled=True)  140 us
    unnamed x4, waiting for transfers between devices  102 us
    all_gather x1, waiting for transfers between devices, dense_shards(): all_both = lax.all_gather(both, all_axes, axis=0, tiled=True)  49.2 us
    all_gather x1, blocking collectives, dense_shards(): all_weights = lax.all_gather(weights, 'ep', axis=0, tiled=True)  32.4 us
    dot_general x1, matrix products, expert_terms(): jnp.einsum('erf,edf->erd', up_pre_grad, up_proj, preferred_element_type=j...  11.4 us
    dot_general x1, matrix products, expert_terms(): jnp.einsum('erf,edf->erd', gate_pre_grad, gate_proj, preferred_element_ty...  9.35 us
  transfers between devices with their start and end apart: 3, of which 3 were waited for; matrix products, arithmetic and copies ran while one was open for 9% of the time, Pallas kernels for 0%

profile of v1, /device:TPU:0, one launch (start us, length us, event | category | flops | bytes accessed | tf_op | source)
XLA Modules:
  0.0 417.0 jit_solution(15202121153911401712)
XLA Ops:
  7.2 0.0 copy-start
  7.2 0.0 all-gather.3.cloned.1.call-start
  7.2 1.0 constant_dynamic-slice_fusion
  8.3 0.7 pad_maximum_fusion
  9.0 0.0 all-gather.3.cloned.1.call-update
  9.0 0.0 reduce-scatter.7.cloned.1.call-start
  9.1 0.7 select_reduce_fusion.1
  9.8 32.4 %all_gather.12 = f32[2048,16]{0,1:T(8,128)S(1)} all-gather(f32[256,16]{0,1:T(8,128)S(1)} %select_reduce_fusion.1), channel_id=1, replica_groups=mesh['ep'=8,'tp'=4] {'ep'}, dimensions={0}, use_global_device_ids=true | all-gather | bytes 147456 | tf_op jit(solution)/shard_map/all_gather | solution.py:141
  42.2 49.2 %all-gather.3.cloned.1.call-done = bf16[2048,2048]{1,0:T(8,128)(2,1)} async-done(((bf16[64,2048]{1,0:T(8,128)(2,1)}), bf16[2048,2048]{1,0:T(8,128)(2,1)}) %all-gather.3.cloned.1.call-update) | async-done | bytes 8388624 | tf_op jit(solution)/shard_map/all_gather | solution.py:138
  91.5 7.5 %fusion.29 = (bf16[2048,1024]{1,0:T(8,128)(2,1)}, f32[2048,1024]{1,0:T(8,128)}) fusion(bf16[2048,2048]{1,0:T(8,128)(2,1)} %all-gather.3.cloned.1.call-done), kind=kLoop, calls=%fused_computation.42 | loop fusion | flops 2097152 | bytes 20971520 | tf_op jit(solution)/shard_map/slice | solution.py:144
  99.0 6.5 %copy.60 = bf16[2048,1024]{0,1:T(8,128)(2,1)} copy(bf16[2048,1024]{1,0:T(8,128)(2,1)} %get-tuple-element.9) | data formatting | bytes 8388608 | tf_op jit(solution)/shard_map/slice | solution.py:144
  105.5 0.0 copy-done.4
  105.5 3.7 fusion.17
  109.2 0.0 copy-done
  109.2 0.0 copy-start.8
  109.2 0.0 slice-start.1
  109.2 0.0 copy-start.7
  109.2 3.9 fusion.14
  113.1 0.0 copy-start.2
  113.2 0.0 copy-done.8
  113.2 0.0 slice-done
  113.2 0.0 slice-done.1
  113.2 0.0 copy-done.7
  113.2 5.0 %multiply_reduce_fusion = (f32[2,2048]{1,0:T(2,128)S(1)}, bf16[2,2048,128]{1,2,0:T(8,128)(2,1)}, f32[2,2048,128]{1,2,0:T(8,128)S(1)}) fusion(bf16[2,2048,128]{1,2,0:T(8,128)(2,1)S(1)} %fusion.17, bf16[2,2048,128]{1,2,0:T(8,128)(2,1)S(1)} %fusion.14, bf16[2,128,1024]{2,1,0:T(8,128)(2,1)S(1)} %copy-done.7, f32[2048,1024]{1,0:T(8,128)S(1)} %bitcast.16, ...), kind=kOutput, calls=%fused_computation.31 | convolution fusion | flops 1090514944 | bytes 14188544 | tf_op jit(solution)/shard_map/erd,efd->erf/dot_general | solution.py:15
  118.2 0.0 copy-done.2
  118.3 1.3 copy.78
  119.6 0.0 reduce-scatter.7.cloned.1.call-update
  119.6 0.2 reduce-scatter.5.cloned.1.call-start
  119.9 9.3 %fusion.30 = f32[2,2048,1024]{2,1,0:T(8,128)} fusion(bf16[2,2048,128]{1,2,0:T(8,128)(2,1)} %get-tuple-element.12, bf16[2,1024,128]{2,1,0:T(8,128)(2,1)S(1)} %copy-done), kind=kOutput, calls=%fused_computation.43 | convolution fusion | flops 1073741824 | bytes 18350080 | tf_op jit(solution)/shard_map/erf,edf->erd/dot_general | solution.py:28
  129.2 11.4 %add_reduce_fusion = f32[2048,1024]{1,0:T(8,128)} fusion(f32[2,2048,1024]{2,1,0:T(8,128)} %fusion.30, bf16[2,1024,128]{2,1,0:T(8,128)(2,1)S(1)} %copy-done.4, f32[2,2048,128]{1,2,0:T(8,128)S(1)} %get-tuple-element.13, bf16[2,2048,128]{1,2,0:T(8,128)(2,1)} %copy-done.2), kind=kOutput, calls=%fused_computation | convolution fusion | flops 1083703296 | bytes 28835840 | tf_op jit(solution)/shard_map/erf,edf->erd/dot_general | solution.py:31
  140.6 0.0 reduce-scatter.5.cloned.1.call-update
  140.7 0.0 copy-start.3
  140.7 0.0 slice-start.2
  140.7 5.9 %fusion.8 = f32[2,1024,128]{2,1,0:T(8,128)} fusion(bf16[2,2048,128]{1,2,0:T(8,128)(2,1)} %get-tuple-element.12, bf16[2048,1024]{0,1:T(8,128)(2,1)} %copy.60), kind=kOutput, calls=%fused_computation.11 | convolution fusion | flops 1073741824 | bytes 6291456 | tf_op jit(solution)/shard_map/erd,erf->edf/dot_general | solution.py:40
  146.6 0.0 copy-done.3
  146.7 3.4 fusion.6
  150.1 0.0 copy-start.5
  150.1 0.0 copy-start.6
  150.1 3.2 fusion
  153.3 102.0 %reduce-scatter.7.cloned.1.call-done = f32[64,16]{1,0:T(8,128)} async-done(((f32[2048,16]{1,0:T(8,128)}), f32[64,16]{1,0:T(8,128)}) %reduce-scatter.7.cloned.1.call-update) | async-done | bytes 4112
  255.3 0.8 copy.79
  256.1 5.2 %all-gather = f32[4,64,16]{1,2,0:T(8,128)S(1)} all-gather(f32[1,64,16]{1,2,0:T(8,128)S(1)} %bitcast.19), channel_id=1, replica_groups=mesh['ep'=8,'tp'=4] {'tp'}, dimensions={0}, use_global_device_ids=true | all-gather | bytes 20480 | tf_op jit(solution)/shard_map/all_gather | solution.py:157
  261.3 0.1 reshape.17
  261.4 0.6 div.7
  262.0 140.2 %reduce-scatter.5.cloned.1.call-done = f32[64,1024]{1,0:T(8,128)} async-done(((f32[2048,1024]{1,0:T(8,128)}), f32[64,1024]{1,0:T(8,128)}) %reduce-scatter.5.cloned.1.call-update) | async-done | bytes 262160 | tf_op jit(solution)/shard_map/reduce_scatter | solution.py:154
  402.2 1.0 convert_element_type.38
  403.2 6.5 %all_gather.14 = bf16[256,1024]{1,0:T(8,128)(2,1)S(1)} all-gather(bf16[64,1024]{1,0:T(8,128)(2,1)S(1)} %convert_element_type.38), channel_id=1, replica_groups=mesh['ep'=8,'tp'=4] {'tp'}, dimensions={0}, use_global_device_ids=true | all-gather | bytes 655360 | tf_op jit(solution)/shard_map/all_gather | solution.py:156
  409.7 0.8 copy.82
  (18 shorter events, 0.1 us)
Async XLA Ops:
  7.2 102.0 %copy-start = (bf16[2,1024,128]{2,1,0:T(8,128)(2,1)S(1)}, bf16[2,1024,128]{2,1,0:T(8,128)(2,1)}, u32[]{:S(2)}) copy-start(bf16[2,1024,128]{2,1,0:T(8,128)(2,1)} %param.11) | copy-start | bytes 1572868
  7.2 84.3 %all-gather.3.cloned.1.call-start = ((), (), s32[]{:S(2)}) async-start(), calls=%async_computation.2 | async-start | bytes 8650752 | tf_op jit(solution)/shard_map/all_gather | solution.py:138
  9.0 246.3 %reduce-scatter.7.cloned.1.call-start = ((), (), s32[]{:S(2)}) async-start(), calls=%async_computation.4 | async-start | bytes 1081344
  99.0 6.6 %copy-start.4 = (bf16[2,1024,128]{2,1,0:T(8,128)(2,1)S(1)}, bf16[2,1024,128]{2,1,0:T(8,128)(2,1)}, u32[]{:S(2)}) copy-start(bf16[2,1024,128]{2,1,0:T(8,128)(2,1)} %param.12) | copy-start | bytes 1572868
  105.5 7.7 %slice-start = ((s8[8388608]{0:T(1024)(128)(4,1)}), s8[4194304]{0:T(1024)(128)(4,1)S(1)}, s32[]{:S(2)}) async-start(s8[8388608]{0:T(1024)(128)(4,1)} %bitcast.15), calls=%async_computation.5 | async-start | bytes 8388608
  109.2 4.0 copy-start.8
  109.2 4.0 slice-start.1
  109.2 4.0 copy-start.7
  113.1 5.1 %copy-start.2 = (bf16[2,2048,128]{1,2,0:T(8,128)(2,1)}, bf16[2,2048,128]{1,2,0:T(8,128)(2,1)S(1)}, u32[]{:S(2)}) copy-start(bf16[2,2048,128]{1,2,0:T(8,128)(2,1)S(1)} %fusion.14) | copy-start | bytes 3145732
  119.6 282.6 %reduce-scatter.5.cloned.1.call-start = ((), (), s32[]{:S(2)}) async-start(), calls=%async_computation.3 | async-start | bytes 8650752 | tf_op jit(solution)/shard_map/reduce_scatter | solution.py:154
  140.7 6.0 %copy-start.1 = (bf16[2048,1024]{0,1:T(8,128)(2,1)S(1)}, bf16[2048,1024]{0,1:T(8,128)(2,1)}, u32[]{:S(2)}) copy-start(bf16[2048,1024]{0,1:T(8,128)(2,1)} %copy.60) | copy-start | bytes 12582916
  140.7 6.0 %copy-start.3 = (bf16[2,2048,128]{1,2,0:T(8,128)(2,1)S(1)}, bf16[2,2048,128]{1,2,0:T(8,128)(2,1)}, u32[]{:S(2)}) copy-start(bf16[2,2048,128]{1,2,0:T(8,128)(2,1)} %copy-done.2) | copy-start | bytes 3145732
  140.7 9.4 %slice-start.2 = ((s8[8388608]{0:T(1024)(128)(4,1)}), s8[4194304]{0:T(1024)(128)(4,1)S(1)}, s32[]{:S(2)}) async-start(s8[8388608]{0:T(1024)(128)(4,1)} %bitcast.17), calls=%async_computation.7 | async-start | bytes 8388608
  146.6 3.4 slice-start.3
  146.6 3.4 copy-start.9
  150.1 111.3 %copy-start.5 = (s32[256,2]{0,1:T(2,128)S(1)}, s32[256,2]{0,1:T(2,128)}, u32[]{:S(2)}) copy-start(s32[256,2]{0,1:T(2,128)} %param.9) | copy-start | bytes 6148
  150.1 111.3 %copy-start.6 = (f32[256,2]{0,1:T(2,128)S(1)}, f32[256,2]{0,1:T(2,128)}, u32[]{:S(2)}) copy-start(f32[256,2]{0,1:T(2,128)} %param.10) | copy-start | bytes 6148
Sparse Core Ops, SparseCore 0:
  11.4 79.9 all-gather.2
  119.7 135.4 reduce-scatter.6
  257.6 144.5 reduce-scatter.4

commit v2 on v0

--- a/solution.py
+++ b/solution.py
@@ -64,22 +64,27 @@
     )
     position = jnp.sum(jnp.cumsum(onehot, axis=0) * onehot, axis=1) - 1
     pair_slot = pair_expert * capacity + position
-    pair_number = jnp.arange(pair_count, dtype=jnp.int32)
-    owner_pair = jnp.zeros((slot_count,), jnp.int32).at[pair_slot].set(pair_number)
-    filled = jnp.zeros((slot_count,), jnp.int32).at[pair_slot].set(1) > 0
-    owner_token = owner_pair // top_count
-    slot_weight = jnp.where(filled, gate_weights.reshape(pair_count)[owner_pair], 0.0)
-    send_rows = jnp.where(filled[:, None], tokens[owner_token], jnp.zeros((), jnp.bfloat16))
-    send_scaled = (slot_weight[:, None] * cotangent[owner_token].astype(jnp.float32)).astype(
-        jnp.bfloat16
-    )
-    layout = (groups, local_experts, capacity, model_width)
-    send_rows = send_rows.reshape(layout)
-    send_scaled = send_scaled.reshape(layout)
+    token_slot = pair_slot.reshape(token_count, top_count)
     quarter = capacity // members
     quarter_start = lax.axis_index("tp") * quarter
-    part_rows = lax.dynamic_slice_in_dim(send_rows, quarter_start, quarter, 2)
-    part_scaled = lax.dynamic_slice_in_dim(send_scaled, quarter_start, quarter, 2)
+    slot_ids = (
+        jnp.arange(experts, dtype=jnp.int32)[:, None] * capacity
+        + quarter_start
+        + jnp.arange(quarter, dtype=jnp.int32)[None, :]
+    ).reshape(experts * quarter)
+    pick = jnp.zeros((experts * quarter, token_count), jnp.bool_)
+    pick_weight = jnp.zeros((experts * quarter, token_count), jnp.float32)
+    for k in range(top_count):
+        match = token_slot[:, k][None, :] == slot_ids[:, None]
+        pick = pick | match
+        pick_weight = jnp.where(match, gate_weights[:, k][None, :], pick_weight)
+    pick = pick.astype(jnp.bfloat16)
+    slot_weight = jnp.sum(pick_weight, axis=1)
+    layout = (groups, local_experts, quarter, model_width)
+    part_rows = jnp.dot(pick, tokens, preferred_element_type=jnp.float32)
+    part_rows = part_rows.astype(jnp.bfloat16).reshape(layout)
+    part_scaled = jnp.dot(pick, cotangent, preferred_element_type=jnp.float32)
+    part_scaled = (slot_weight[:, None] * part_scaled).astype(jnp.bfloat16).reshape(layout)
     landed = (
         lax.all_to_all(part_rows, "ep", split_axis=0, concat_axis=0, tiled=True),
         lax.all_to_all(part_scaled, "ep", split_axis=0, concat_axis=0, tiled=True),
@@ -97,22 +102,29 @@
     input_grad, product, gate_grad, up_grad, down_grad = expert_terms(
         expert_rows, expert_scaled, gate_proj, up_proj, down_proj
     )
-    input_grad = input_grad.reshape(local_experts, groups, capacity, model_width).transpose(
-        1, 0, 2, 3
+    peak = jnp.maximum(jnp.max(jnp.abs(input_grad), axis=-1), 1e-30)
+    narrow = (input_grad * (1.0 / peak)[:, :, None]).astype(jnp.float16)
+    narrow = narrow.reshape(local_experts, groups, capacity, model_width).transpose(1, 0, 2, 3)
+    extras = jnp.stack([product, peak])
+    extras = extras.reshape(2, local_experts, groups, capacity).transpose(2, 0, 1, 3)
+    back_narrow, back_extras = (
+        lax.all_to_all(narrow, "ep", split_axis=0, concat_axis=0, tiled=True),
+        lax.all_to_all(extras, "ep", split_axis=0, concat_axis=0, tiled=True),
     )
-    product = product.reshape(local_experts, groups, capacity).transpose(1, 0, 2)
-    back_grad, back_product = (
-        lax.all_to_all(input_grad, "ep", split_axis=0, concat_axis=0, tiled=True),
-        lax.all_to_all(product, "ep", split_axis=0, concat_axis=0, tiled=True),
+    back_product = back_extras[:, 0].reshape(slot_count)
+    back_peak = back_extras[:, 1].reshape(slot_count)
+    back_grad = back_narrow.reshape(slot_count, model_width).astype(jnp.float32) * back_peak[:, None]
+    coarse = lax.reduce_precision(back_grad, 8, 7)
+    fine = (back_grad - coarse).astype(jnp.bfloat16)
+    coarse = coarse.astype(jnp.bfloat16)
+    all_slots = jnp.arange(slot_count, dtype=jnp.int32)
+    slot_match = token_slot[:, :, None] == all_slots[None, None, :]
+    spread = jnp.any(slot_match, axis=1).astype(jnp.bfloat16)
+    token_grad = jnp.dot(spread, coarse, preferred_element_type=jnp.float32) + jnp.dot(
+        spread, fine, preferred_element_type=jnp.float32
     )
-    local_slot = position
-    present = (local_slot >= 0) & (local_slot < capacity)
-    back_index = pair_expert * capacity + jnp.clip(local_slot, 0, capacity - 1)
-    pair_grad = jnp.where(
-        present[:, None], back_grad.reshape(experts * capacity, model_width)[back_index], 0.0
-    )
-    pair_product = jnp.where(present, back_product.reshape(experts * capacity)[back_index], 0.0)
-    token_grad = jnp.sum(pair_grad.reshape(token_count, top_count, model_width), axis=1)
+    pair_product = jnp.sum(jnp.where(slot_match, back_product[None, None, :], 0.0), axis=2)
+    pair_product = pair_product.reshape(pair_count)
     total_grad, total_product = lax.psum((token_grad, pair_product), "tp")
     tokens_grad = total_grad.astype(jnp.bfloat16)
     gates_grad = (total_product / gate_weights.reshape(pair_count)).reshape(token_count, top_count)

time: 328 us -> 241 us (0.73)
  waiting for transfers between devices: 151 us -> 90 us
  local copies, waits for them, and re-layouts: 50.8 us -> 15 us
  matrix products: 14.3 us -> 25.3 us
    all_to_all x2, waiting for transfers between devices: 127 us -> 60.8 us  [the longest x1 60.3 us: shards(): lax.all_to_all(narrow, 'ep', split_axis=0, concat_axis=0, tiled=True)]
    gather x6 -> x0, local copies, waits for them, and re-layouts: 32.1 us -> none  [the longest x1 9.48 us: shards(): gate_weights.reshape(pair_count)[owner_pair]]
    all_gather x1, waiting for transfers between devices: 0.02 us -> 26 us  [shards(): lax.all_gather(landed[0], 'tp', axis=2, tiled=True)]
    all_gather x1, waiting for transfers between devices: 23.6 us -> 3.17 us  [shards(): lax.all_gather(landed[1], 'tp', axis=2, tiled=True)]
    dot_general x0 -> x4, matrix products: none -> 8.1 us  [the longest x1 3.26 us: shards(): jnp.dot(spread, fine, preferred_element_type=jnp.float32)]
    scatter x2 -> x0, local copies, waits for them, and re-layouts: 4.9 us -> none  [the longest x1 2.45 us: shards(): jnp.zeros((slot_count,), jnp.int32).at[pair_slot].set(pair_number)]
    all_to_all x1, blocking collectives: 23.5 us -> 27.8 us  [shards(): lax.all_to_all(part_scaled, 'ep', split_axis=0, concat_axis=0, tiled=True)]
    all_to_all x1, blocking collectives: 27.8 us -> 23.6 us  [shards(): lax.all_to_all(part_rows, 'ep', split_axis=0, concat_axis=0, tiled=True)]
  transfers between devices with their start and end apart: 4 -> 4, of which waited for: 3 -> 4; matrix products, arithmetic and copies ran while one was open for 9% -> 9% of each run, Pallas kernels for 0% -> 0%
where the time goes in v2:
time: 241 us; the launch traced here: 240 us
  waiting for transfers between devices  90 us (37%)
  blocking collectives  77.4 us (32%)
  matrix products  25.3 us (10%)
  local copies, waits for them, and re-layouts  15 us (6%)
  between operations  14.3 us (6%)
  starting transfers between devices  11.2 us (5%)
  other arithmetic  6.69 us (3%)
    all_to_all x1, waiting for transfers between devices, shards(): lax.all_to_all(narrow, 'ep', split_axis=0, concat_axis=0, tiled=True)  60.3 us
    all_to_all x1, blocking collectives, shards(): lax.all_to_all(part_scaled, 'ep', split_axis=0, concat_axis=0, tiled=True)  27.8 us
    psum x1, blocking collectives, shards(): total_grad, total_product = lax.psum((token_grad, pair_product), 'tp')  26 us
    all_gather x1, waiting for transfers between devices, shards(): lax.all_gather(landed[0], 'tp', axis=2, tiled=True)  26 us
    all_to_all x1, blocking collectives, shards(): lax.all_to_all(part_rows, 'ep', split_axis=0, concat_axis=0, tiled=True)  23.6 us
    all_to_all x1, starting transfers between devices, shards(): lax.all_to_all(narrow, 'ep', split_axis=0, concat_axis=0, tiled=True)  5.57 us
    all_to_all x1, starting transfers between devices, shards(): lax.all_to_all(extras, 'ep', split_axis=0, concat_axis=0, tiled=True)  5.52 us
  transfers between devices with their start and end apart: 4, of which 4 were waited for; matrix products, arithmetic and copies ran while one was open for 9% of the time, Pallas kernels for 0%

profile of v2, /device:TPU:0, one launch (start us, length us, event | category | flops | bytes accessed | tf_op | source)
XLA Modules:
  0.0 239.9 jit_solution(1141995513742592962)
XLA Ops:
  7.2 0.9 copy.101
  8.1 0.1 eq.70
  8.3 0.1 eq.66
  8.5 0.8 fusion.33
  9.4 1.2 reduce-window.6
  10.5 0.2 slice_reduce_fusion
  10.8 0.1 fusion.28
  10.9 0.1 sub.13
  11.1 0.7 multiply_add_fusion
  11.8 0.2 fusion.18
  12.1 1.5 multiply_convert_fusion.1
  13.5 27.8 %all_to_all.20 = bf16[8,2,24,1024]{3,2,1,0:T(8,128)(2,1)} all-to-all(bf16[8,2,24,1024]{3,2,1,0:T(8,128)(2,1)S(1)} %bitcast.61), channel_id=1, replica_groups=mesh['ep'=8,'tp'=4] {'ep'}, dimensions={0} | all-to-all | bytes 1572864 | tf_op jit(solution)/shard_map/all_to_all | solution.py:90
  41.4 0.4 convolution_convert_fusion
  41.8 23.6 %all_to_all.21 = bf16[8,2,24,1024]{3,2,1,0:T(8,128)(2,1)} all-to-all(bf16[8,2,24,1024]{3,2,1,0:T(8,128)(2,1)S(1)} %bitcast.60), channel_id=1, replica_groups=mesh['ep'=8,'tp'=4] {'ep'}, dimensions={0} | all-to-all | bytes 1572864 | tf_op jit(solution)/shard_map/all_to_all | solution.py:89
  65.4 3.2 %all-gather.3.cloned.1.call-done = bf16[8,2,96,1024]{3,2,1,0:T(8,128)(2,1)} async-done(((bf16[8,2,24,1024]{3,2,1,0:T(8,128)(2,1)}), bf16[8,2,96,1024]{3,2,1,0:T(8,128)(2,1)}) %all-gather.3.cloned.1.call-update) | async-done | bytes 3145744 | tf_op jit(solution)/shard_map/all_gather | solution.py:94
  68.6 4.0 %copy.105 = bf16[2,8,96,1024]{3,2,1,0:T(8,128)(2,1)} copy(bf16[2,8,96,1024]{3,2,0,1:T(8,128)(2,1)} %bitcast.58) | data formatting | bytes 6291456 | tf_op jit(solution)/shard_map/transpose | solution.py:99
  72.6 26.0 %all-gather.5.cloned.1.call-done = bf16[8,2,96,1024]{3,2,1,0:T(8,128)(2,1)} async-done(((bf16[8,2,24,1024]{3,2,1,0:T(8,128)(2,1)}), bf16[8,2,96,1024]{3,2,1,0:T(8,128)(2,1)}) %all-gather.5.cloned.1.call-update) | async-done | bytes 3145744 | tf_op jit(solution)/shard_map/all_gather | solution.py:93
  98.6 2.3 copy.106
  101.0 1.2 convolution_convert_fusion.1
  102.1 0.2 copy-done.5
  102.3 1.2 convolution_convert_fusion.2
  103.5 0.6 copy-done.3
  104.1 0.1 copy-done.8
  104.2 1.4 multiply_reduce_fusion
  105.6 1.0 fusion.34
  106.7 3.9 %abs_reduce_fusion = (f32[2,768]{1,0:T(2,128)S(1)}, f32[2,768,1024]{2,1,0:T(8,128)}) fusion(f32[2,768,1024]{2,1,0:T(8,128)S(1)} %fusion.34, bf16[2,1024,128]{2,1,0:T(8,128)(2,1)S(1)} %copy-done, f32[2,768,128]{1,2,0:T(8,128)S(1)} %get-tuple-element.46, bf16[2,768,128]{1,2,0:T(8,128)(2,1)S(1)} %convolution_convert_fusion.2), kind=kOutput, calls=%fused_computation.5 | convolution fusion | flops 408746496 | bytes 14292992 | tf_op jit(solution)/shard_map/erf,edf->erd/dot_general | solution.py:31
  110.6 0.6 copy.112
  111.3 5.5 %all-to-all-start.3 = ((f32[8,2,2,96]{3,2,1,0:T(2,128)}), f32[8,2,2,96]{3,2,1,0:T(2,128)S(1)}, u32[]{:S(2)}, u32[]{:S(2)}) async-start(f32[8,2,2,96]{3,2,1,0:T(2,128)} %copy.112), calls=%async_computation.3 | async-start | bytes 32768 | tf_op jit(solution)/shard_map/all_to_all | solution.py:112
  116.8 3.4 %multiply_convert_fusion = f16[2,768,1024]{2,1,0:T(8,128)(2,1)S(1)} fusion(f32[2,768,1024]{2,1,0:T(8,128)} %get-tuple-element.48, f32[2,768]{1,0:T(2,128)S(1)} %get-tuple-element.41), kind=kLoop, calls=%fused_computation.4 | loop fusion | flops 3145728 | bytes 9443328 | tf_op jit(solution)/shard_map/convert_element_type | solution.py:106
  120.1 2.6 %copy.131 = f16[2,8,96,1024]{3,2,0,1:T(8,128)(2,1)} copy(f16[2,8,96,1024]{3,2,1,0:T(8,128)(2,1)S(1)} %bitcast.55) | data formatting | bytes 6291456 | tf_op jit(solution)/shard_map/reshape | solution.py:107
  122.8 0.6 all-to-all-done.3
  123.4 5.6 %all-to-all-start.2 = ((f16[8,2,96,1024]{3,2,1,0:T(8,128)(2,1)}), f16[8,2,96,1024]{3,2,1,0:T(8,128)(2,1)}, u32[]{:S(2)}, u32[]{:S(2)}) async-start(f16[8,2,96,1024]{3,2,1,0:T(8,128)(2,1)} %bitcast.54), calls=%async_computation.2 | async-start | bytes 6291456 | tf_op jit(solution)/shard_map/all_to_all | solution.py:111
  128.9 0.1 copy.114
  129.1 0.1 reshape.122
  129.2 0.5 fusion.6
  129.7 4.5 %fusion.35 = f32[2,1024,128]{2,1,0:T(8,128)} fusion(bf16[2,768,1024]{2,1,0:T(8,128)(2,1)} %bitcast.52, bf16[2,768,128]{1,2,0:T(8,128)(2,1)S(1)} %get-tuple-element.37), kind=kOutput, calls=%fused_computation.66 | convolution fusion | flops 402653184 | bytes 4587520 | tf_op jit(solution)/shard_map/erd,erf->edf/dot_general | solution.py:40
  134.2 1.8 fusion.19
  136.0 0.4 copy-done.2
  136.4 2.4 fusion.30
  138.9 0.5 select_reduce_fusion
  139.4 0.1 copy.113
  139.6 0.1 reshape.121
  139.7 60.3 %all-to-all-done.2 = f16[8,2,96,1024]{3,2,1,0:T(8,128)(2,1)} async-done(((f16[8,2,96,1024]{3,2,1,0:T(8,128)(2,1)}), f16[8,2,96,1024]{3,2,1,0:T(8,128)(2,1)}, u32[]{:S(2)}, u32[]{:S(2)}) %all-to-all-start.2) | async-done | bytes 3145760 | tf_op jit(solution)/shard_map/all_to_all | solution.py:111
  200.0 3.0 %fusion.3 = f32[256,1024]{1,0:T(8,128)S(1)} fusion(pred[256,1536]{1,0:T(8,128)(4,1)S(1)} %fusion.6, f16[1536,1024]{1,0:T(8,128)(2,1)} %bitcast.15, f32[1536]{0:T(1024)S(1)} %mul.90), kind=kOutput, calls=%fused_computation.7 | convolution fusion | flops 811597824 | bytes 4593664 | tf_op jit(solution)/shard_map/dot_general | solution.py:123
  202.9 3.3 %fusion.7 = f32[256,1024]{1,0:T(8,128)S(1)} fusion(f32[256,1024]{1,0:T(8,128)S(1)} %fusion.3, pred[256,1536]{1,0:T(8,128)(4,1)S(1)} %fusion.6, f16[1536,1024]{1,0:T(8,128)(2,1)} %bitcast.15, f32[1536]{0:T(1024)S(1)} %mul.90), kind=kOutput, calls=%fused_computation.17 | convolution fusion | flops 813432832 | bytes 5642240 | tf_op jit(solution)/shard_map/dot_general | solution.py:123
  206.2 26.0 %all-reduce.2 = (bf16[256,1024]{1,0:T(8,128)(2,1)}, f32[512]{0:T(512)S(1)}) all-reduce(f32[256,1024]{1,0:T(8,128)S(1)} %fusion.7, f32[512]{0:T(512)S(1)} %reshape.121), channel_id=1, replica_groups=mesh['ep'=8,'tp'=4] {'tp'}, use_global_device_ids=true, to_apply=%region_7.8 | all-reduce | flops 262656 | bytes 1576960 | tf_op jit(solution)/shard_map/psum | solution.py:128
  232.3 0.1 reshape.123
  232.4 0.7 copy.119
  (35 shorter events, 0.8 us)
Async XLA Ops:
  7.2 93.8 %copy-start = (bf16[2,1024,128]{2,1,0:T(8,128)(2,1)S(1)}, bf16[2,1024,128]{2,1,0:T(8,128)(2,1)}, u32[]{:S(2)}) copy-start(bf16[2,1024,128]{2,1,0:T(8,128)(2,1)} %param.12) | copy-start | bytes 1572868
  7.2 34.2 %copy-start.6 = (bf16[256,1024]{1,0:T(8,128)(2,1)S(1)}, bf16[256,1024]{1,0:T(8,128)(2,1)}, u32[]{:S(2)}) copy-start(bf16[256,1024]{1,0:T(8,128)(2,1)} %param.7) | copy-start | bytes 1572868
  7.2 61.4 %all-gather.3.cloned.1.call-start = ((), (), s32[]{:S(2)}) async-start(), calls=%async_computation.4 | async-start | bytes 3932160 | tf_op jit(solution)/shard_map/all_gather | solution.py:94
  41.4 57.2 %all-gather.5.cloned.1.call-start = ((), (), s32[]{:S(2)}) async-start(), calls=%async_computation.5 | async-start | bytes 3932160 | tf_op jit(solution)/shard_map/all_gather | solution.py:93
  100.9 2.6 %copy-start.1 = (bf16[2,8,96,1024]{3,2,1,0:T(8,128)(2,1)}, bf16[2,8,96,1024]{3,2,1,0:T(8,128)(2,1)S(1)}, u32[]{:S(2)}) copy-start(bf16[2,8,96,1024]{3,2,1,0:T(8,128)(2,1)S(1)} %copy.106) | copy-start | bytes 9437188
  100.9 1.4 copy-start.5
  100.9 3.2 %copy-start.3 = (bf16[2,8,96,1024]{3,2,1,0:T(8,128)(2,1)S(1)}, bf16[2,8,96,1024]{3,2,1,0:T(8,128)(2,1)}, u32[]{:S(2)}) copy-start(bf16[2,8,96,1024]{3,2,1,0:T(8,128)(2,1)} %copy.105) | copy-start | bytes 9437188
  100.9 3.3 %copy-start.8 = (bf16[2,128,1024]{2,1,0:T(8,128)(2,1)S(1)}, bf16[2,128,1024]{2,1,0:T(8,128)(2,1)}, u32[]{:S(2)}) copy-start(bf16[2,128,1024]{2,1,0:T(8,128)(2,1)} %param.13) | copy-start | bytes 1572868
  111.3 12.1 %all-to-all-start.3 = ((f32[8,2,2,96]{3,2,1,0:T(2,128)}), f32[8,2,2,96]{3,2,1,0:T(2,128)S(1)}, u32[]{:S(2)}, u32[]{:S(2)}) async-start(f32[8,2,2,96]{3,2,1,0:T(2,128)} %copy.112), calls=%async_computation.3 | async-start | bytes 32768 | tf_op jit(solution)/shard_map/all_to_all | solution.py:112
  123.4 5.6 %copy-start.7 = (f32[256,2]{0,1:T(2,128)S(1)}, f32[256,2]{0,1:T(2,128)}, u32[]{:S(2)}) copy-start(f32[256,2]{0,1:T(2,128)} %param.10) | copy-start | bytes 6148
  123.4 76.6 %all-to-all-start.2 = ((f16[8,2,96,1024]{3,2,1,0:T(8,128)(2,1)}), f16[8,2,96,1024]{3,2,1,0:T(8,128)(2,1)}, u32[]{:S(2)}, u32[]{:S(2)}) async-start(f16[8,2,96,1024]{3,2,1,0:T(8,128)(2,1)} %bitcast.54), calls=%async_computation.2 | async-start | bytes 6291456 | tf_op jit(solution)/shard_map/all_to_all | solution.py:111
  129.2 5.0 %copy-start.4 = (bf16[2,8,96,1024]{3,2,1,0:T(8,128)(2,1)S(1)}, bf16[2,8,96,1024]{3,2,1,0:T(8,128)(2,1)}, u32[]{:S(2)}) copy-start(bf16[2,8,96,1024]{3,2,1,0:T(8,128)(2,1)} %copy.105) | copy-start | bytes 9437188
  134.2 2.2 copy-start.2
Sparse Core Ops, SparseCore 0:
  41.5 27.0 all-gather.2
  70.2 28.3 all-gather.4

commit v3 on v2

--- a/solution.py
+++ b/solution.py
@@ -44,6 +44,11 @@
         "erd,erf->edf", expert_rows, up_pre_grad, preferred_element_type=jnp.float32
     )
     return (input_grad, product, gate_grad, up_grad, down_grad)
+
+
+def narrowed(values):
+    peak = jnp.maximum(jnp.max(jnp.abs(values), axis=-1), 1e-30)
+    return (values * (1.0 / peak)[:, :, None]).astype(jnp.float16), peak
 
 
 def shards(tokens, cotangent, routing, gate_weights, gate_proj, up_proj, down_proj):
@@ -102,9 +107,18 @@
     input_grad, product, gate_grad, up_grad, down_grad = expert_terms(
         expert_rows, expert_scaled, gate_proj, up_proj, down_proj
     )
-    peak = jnp.maximum(jnp.max(jnp.abs(input_grad), axis=-1), 1e-30)
-    narrow = (input_grad * (1.0 / peak)[:, :, None]).astype(jnp.float16)
-    narrow = narrow.reshape(local_experts, groups, capacity, model_width).transpose(1, 0, 2, 3)
+    half = model_width // 2
+    parity = lax.axis_index("tp") % 2
+    twins = [(member, member ^ 1) for member in range(members)]
+    own = lax.dynamic_slice_in_dim(input_grad, parity * half, half, 2)
+    other = lax.dynamic_slice_in_dim(input_grad, (1 - parity) * half, half, 2)
+    other_narrow, other_peak = narrowed(other)
+    twin_narrow = lax.ppermute(other_narrow, "tp", twins)
+    twin_extras = lax.ppermute(jnp.stack([product, other_peak]), "tp", twins)
+    own = own + twin_narrow.astype(jnp.float32) * twin_extras[1][:, :, None]
+    product = product + twin_extras[0]
+    narrow, peak = narrowed(own)
+    narrow = narrow.reshape(local_experts, groups, capacity, half).transpose(1, 0, 2, 3)
     extras = jnp.stack([product, peak])
     extras = extras.reshape(2, local_experts, groups, capacity).transpose(2, 0, 1, 3)
     back_narrow, back_extras = (
@@ -113,7 +127,7 @@
     )
     back_product = back_extras[:, 0].reshape(slot_count)
     back_peak = back_extras[:, 1].reshape(slot_count)
-    back_grad = back_narrow.reshape(slot_count, model_width).astype(jnp.float32) * back_peak[:, None]
+    back_grad = back_narrow.reshape(slot_count, half).astype(jnp.float32) * back_peak[:, None]
     coarse = lax.reduce_precision(back_grad, 8, 7)
     fine = (back_grad - coarse).astype(jnp.bfloat16)
     coarse = coarse.astype(jnp.bfloat16)
@@ -125,8 +139,18 @@
     )
     pair_product = jnp.sum(jnp.where(slot_match, back_product[None, None, :], 0.0), axis=2)
     pair_product = pair_product.reshape(pair_count)
-    total_grad, total_product = lax.psum((token_grad, pair_product), "tp")
-    tokens_grad = total_grad.astype(jnp.bfloat16)
+    total_grad, total_product = token_grad, pair_product
+    for step in range(2, members, 2):
+        across = [(member, (member + step) % members) for member in range(members)]
+        total_grad = total_grad + lax.ppermute(token_grad, "tp", across)
+        total_product = total_product + lax.ppermute(pair_product, "tp", across)
+    own_half = total_grad.astype(jnp.bfloat16)
+    twin_half = lax.ppermute(own_half, "tp", twins)
+    tokens_grad = jnp.where(
+        parity == 0,
+        jnp.concatenate([own_half, twin_half], axis=1),
+        jnp.concatenate([twin_half, own_half], axis=1),
+    )
     gates_grad = (total_product / gate_weights.reshape(pair_count)).reshape(token_count, top_count)
     return (tokens_grad, gates_grad, gate_grad, up_grad, down_grad)
 

time: 241 us -> 199 us (0.83)
  blocking collectives: 77.4 us -> 51.4 us
  waiting for transfers between devices: 90 us -> 73.3 us
  other arithmetic: 6.69 us -> 11.8 us
  matrix products: 25.3 us -> 20.9 us
    all_to_all x1, waiting for transfers between devices: 60.3 us -> 31.4 us  [shards(): lax.all_to_all(narrow, 'ep', split_axis=0, concat_axis=0, tiled=True)]
    psum x1 -> x0, blocking collectives: 26 us -> none  [shards(): total_grad, total_product = lax.psum((token_grad, pair_product), 'tp')]
    ppermute x0 -> x5, waiting for transfers between devices: none -> 10.2 us  [the longest x1 7.1 us: shards(): total_grad = total_grad + lax.ppermute(token_grad, 'tp', across)]
    reduce_max x0 -> x2, other arithmetic: none -> 3.01 us  [narrowed(): peak = jnp.maximum(jnp.max(jnp.abs(values), axis=-1), 1e-30)]
    dot_general x1, matrix products: 3.86 us -> 1.06 us  [expert_terms(): jnp.einsum('erf,edf->erd', up_pre_grad, up_proj, preferred_element_type=j...]
    ppermute x0 -> x5, starting transfers between devices: none -> 2.74 us  [the longest x1 1.51 us: shards(): total_product = total_product + lax.ppermute(pair_product, 'tp', across)]
    dot_general x1, matrix products: 3.26 us -> 0.84 us  [shards(): jnp.dot(spread, fine, preferred_element_type=jnp.float32)]
  transfers between devices with their start and end apart: 4 -> 9, of which waited for: 4 -> 6; matrix products, arithmetic and copies ran while one was open for 9% -> 11% of each run, Pallas kernels for 0% -> 0%
where the time goes in v3:
time: 199 us; the launch traced here: 198 us
  waiting for transfers between devices  73.3 us (37%)
  blocking collectives  51.4 us (26%)
  matrix products  20.9 us (11%)
  between operations  14.4 us (7%)
  local copies, waits for them, and re-layouts  14.3 us (7%)
  starting transfers between devices  12.1 us (6%)
  other arithmetic  11.8 us (6%)
    all_to_all x1, waiting for transfers between devices, shards(): lax.all_to_all(narrow, 'ep', split_axis=0, concat_axis=0, tiled=True)  31.4 us
    all_to_all x1, blocking collectives, shards(): lax.all_to_all(part_scaled, 'ep', split_axis=0, concat_axis=0, tiled=True)  27.8 us
    all_gather x1, waiting for transfers between devices, shards(): lax.all_gather(landed[0], 'tp', axis=2, tiled=True)  26 us
    all_to_all x1, blocking collectives, shards(): lax.all_to_all(part_rows, 'ep', split_axis=0, concat_axis=0, tiled=True)  23.6 us
    ppermute x1, waiting for transfers between devices, shards(): total_grad = total_grad + lax.ppermute(token_grad, 'tp', across)  7.1 us
    all_to_all x1, starting transfers between devices, shards(): lax.all_to_all(extras, 'ep', split_axis=0, concat_axis=0, tiled=True)  5.52 us
    dot_general x1, matrix products, expert_terms(): jnp.einsum('erd,erf->edf', expert_rows, up_pre_grad, preferred_element_ty...  4.54 us
    convert_element_type x2, other arithmetic, narrowed(): return ((values * (1.0 / peak)[:, :, None]).astype(jnp.float16), peak)  4.45 us
  transfers between devices with their start and end apart: 9, of which 6 were waited for; matrix products, arithmetic and copies ran while one was open for 11% of the time, Pallas kernels for 0%

profile of v3, /device:TPU:0, one launch (start us, length us, event | category | flops | bytes accessed | tf_op | source)
XLA Modules:
  0.0 198.3 jit_solution(13569412484557745164)
XLA Ops:
  7.2 0.9 copy.101
  8.5 0.8 fusion.31
  9.4 1.2 reduce-window.6
  10.5 0.2 slice_reduce_fusion
  11.1 0.7 multiply_add_fusion.1
  11.8 0.2 fusion.16
  12.1 1.5 multiply_convert_fusion.2
  13.5 27.8 %all_to_all.20 = bf16[8,2,24,1024]{3,2,1,0:T(8,128)(2,1)} all-to-all(bf16[8,2,24,1024]{3,2,1,0:T(8,128)(2,1)S(1)} %bitcast.68), channel_id=1, replica_groups=mesh['ep'=8,'tp'=4] {'ep'}, dimensions={0} | all-to-all | bytes 1572864 | tf_op jit(solution)/shard_map/all_to_all | solution.py:95
  41.4 0.4 convolution_convert_fusion
  41.8 23.6 %all_to_all.21 = bf16[8,2,24,1024]{3,2,1,0:T(8,128)(2,1)} all-to-all(bf16[8,2,24,1024]{3,2,1,0:T(8,128)(2,1)S(1)} %bitcast.65), channel_id=1, replica_groups=mesh['ep'=8,'tp'=4] {'ep'}, dimensions={0} | all-to-all | bytes 1572864 | tf_op jit(solution)/shard_map/all_to_all | solution.py:94
  65.4 3.2 %all-gather.3.cloned.1.call-done = bf16[8,2,96,1024]{3,2,1,0:T(8,128)(2,1)} async-done(((bf16[8,2,24,1024]{3,2,1,0:T(8,128)(2,1)}), bf16[8,2,96,1024]{3,2,1,0:T(8,128)(2,1)}) %all-gather.3.cloned.1.call-update) | async-done | bytes 3145744 | tf_op jit(solution)/shard_map/all_gather | solution.py:99
  68.6 4.0 %copy.105 = bf16[2,8,96,1024]{3,2,1,0:T(8,128)(2,1)} copy(bf16[2,8,96,1024]{3,2,0,1:T(8,128)(2,1)} %bitcast.63) | data formatting | bytes 6291456 | tf_op jit(solution)/shard_map/transpose | solution.py:104
  72.6 26.0 %all-gather.5.cloned.1.call-done = bf16[8,2,96,1024]{3,2,1,0:T(8,128)(2,1)} async-done(((bf16[8,2,24,1024]{3,2,1,0:T(8,128)(2,1)}), bf16[8,2,96,1024]{3,2,1,0:T(8,128)(2,1)}) %all-gather.5.cloned.1.call-update) | async-done | bytes 3145744 | tf_op jit(solution)/shard_map/all_gather | solution.py:98
  98.6 2.4 %copy.106 = bf16[2,8,96,1024]{3,2,1,0:T(8,128)(2,1)S(1)} copy(bf16[2,8,96,1024]{3,2,0,1:T(8,128)(2,1)} %bitcast.64) | data formatting | bytes 6291456 | tf_op jit(solution)/shard_map/transpose | solution.py:101
  101.0 1.2 convolution_convert_fusion.1
  102.2 1.2 convolution_convert_fusion.2
  103.4 0.7 copy-done.3
  104.3 1.4 multiply_reduce_fusion
  105.6 1.0 fusion.32
  106.7 1.1 convolution_add_fusion
  107.8 0.3 abs_reduce_fusion.1
  108.1 1.9 multiply_convert_fusion.1
  110.1 0.8 copy-done.1
  110.8 0.2 collective-permute-start
  111.1 0.3 collective-permute-start.1
  111.3 3.1 %collective-permute-done.1 = f32[2,2,768]{2,1,0:T(2,128)S(1)} collective-permute-done((f32[2,2,768]{2,1,0:T(2,128)S(1)}, f32[2,2,768]{2,1,0:T(2,128)S(1)}, u32[]{:S(2)}, u32[]{:S(2)}) %collective-permute-start.1) | collective-permute-done | bytes 12320 | tf_op jit(solution)/shard_map/ppermute | solution.py:117
  114.6 2.7 %abs_reduce_fusion = f32[2,768]{1,0:T(2,128)S(1)} fusion(f16[2,768,512]{2,1,0:T(8,128)(2,1)S(1)} %collective-permute-done, f32[2,768,1024]{2,1,0:T(8,128)} %copy-done.1, s32[]{:T(128)S(6)} %select_n.36, f32[2,768]{1,0:T(2,128)S(1)} %get-tuple-element.39), kind=kLoop, calls=%fused_computation.6 | loop fusion | flops 3930624 | bytes 4730884 | tf_op jit(solution)/shard_map/reduce_max | solution.py:50
  117.3 0.6 copy.112
  118.0 5.5 %all-to-all-start.3 = ((f32[8,2,2,96]{3,2,1,0:T(2,128)}), f32[8,2,2,96]{3,2,1,0:T(2,128)S(1)}, u32[]{:S(2)}, u32[]{:S(2)}) async-start(f32[8,2,2,96]{3,2,1,0:T(2,128)} %copy.112), calls=%async_computation.3 | async-start | bytes 32768 | tf_op jit(solution)/shard_map/all_to_all | solution.py:126
  123.5 2.5 %multiply_convert_fusion = f16[2,768,512]{2,1,0:T(8,128)(2,1)S(1)} fusion(f16[2,768,512]{2,1,0:T(8,128)(2,1)S(1)} %collective-permute-done, f32[2,768,1024]{2,1,0:T(8,128)} %copy-done.1, s32[]{:T(128)S(6)} %select_n.36, f32[2,768]{1,0:T(2,128)S(1)} %get-tuple-element.41, f32[2,768]{1,0:T(2,128)S(1)} %get-tuple-element.39), kind=kLoop, calls=%fused_computation.5 | loop fusion | flops 3932160 | bytes 6303748 | tf_op jit(solution)/shard_map/convert_element_type | solution.py:51
  126.0 1.5 copy.131
  127.5 2.5 %all-to-all-done.3 = f32[8,2,2,96]{3,2,1,0:T(2,128)S(1)} async-done(((f32[8,2,2,96]{3,2,1,0:T(2,128)}), f32[8,2,2,96]{3,2,1,0:T(2,128)S(1)}, u32[]{:S(2)}, u32[]{:S(2)}) %all-to-all-start.3) | async-done | bytes 12320 | tf_op jit(solution)/shard_map/all_to_all | solution.py:126
  130.1 3.8 %all-to-all-start.2 = ((f16[8,2,96,512]{3,2,1,0:T(8,128)(2,1)}), f16[8,2,96,512]{3,2,1,0:T(8,128)(2,1)S(1)}, u32[]{:S(2)}, u32[]{:S(2)}) async-start(f16[8,2,96,512]{3,2,1,0:T(8,128)(2,1)} %bitcast.55), calls=%async_computation.2 | async-start | bytes 3145728 | tf_op jit(solution)/shard_map/all_to_all | solution.py:125
  134.0 0.1 reshape.136
  134.1 0.5 fusion.1
  134.7 4.5 %fusion.28 = f32[2,1024,128]{2,1,0:T(8,128)} fusion(bf16[2,768,1024]{2,1,0:T(8,128)(2,1)} %bitcast.58, f32[2,768,128]{1,2,0:T(8,128)} %copy-done.6, bf16[2,768,128]{1,2,0:T(8,128)(2,1)S(1)} %convolution_convert_fusion.2), kind=kOutput, calls=%fused_computation.72 | convolution fusion | flops 404029440 | bytes 5373952 | tf_op jit(solution)/shard_map/erd,erf->edf/dot_general | solution.py:43
  139.3 31.4 %all-to-all-done.2 = f16[8,2,96,512]{3,2,1,0:T(8,128)(2,1)S(1)} async-done(((f16[8,2,96,512]{3,2,1,0:T(8,128)(2,1)}), f16[8,2,96,512]{3,2,1,0:T(8,128)(2,1)S(1)}, u32[]{:S(2)}, u32[]{:S(2)}) %all-to-all-start.2) | async-done | bytes 1572896 | tf_op jit(solution)/shard_map/all_to_all | solution.py:125
  170.7 0.8 fusion.2
  171.5 1.8 fusion.7
  173.4 0.6 collective-permute-start.2
  174.0 1.8 fusion.17
  175.9 0.5 select_reduce_fusion
  176.6 0.1 reshape.135
  176.7 1.5 collective-permute-start.4
  178.2 7.1 %collective-permute-done.2 = f32[256,512]{1,0:T(8,128)S(1)} collective-permute-done((f32[256,512]{1,0:T(8,128)S(1)}, f32[256,512]{1,0:T(8,128)S(1)}, u32[]{:S(2)}, u32[]{:S(2)}) %collective-permute-start.2) | collective-permute-done | bytes 524320 | tf_op jit(solution)/shard_map/ppermute | solution.py:145
  185.5 4.2 %fusion.33 = f32[2,1024,128]{2,1,0:T(8,128)} fusion(bf16[2,768,1024]{2,1,0:T(8,128)(2,1)} %bitcast.59, bf16[2,768,128]{1,2,0:T(8,128)(2,1)S(1)} %get-tuple-element.35), kind=kOutput, calls=%fused_computation.77 | convolution fusion | flops 402653184 | bytes 4587520 | tf_op jit(solution)/shard_map/erd,erf->edf/dot_general | solution.py:40
  189.8 0.7 copy.119
  190.5 0.9 maximum_select_fusion
  (60 shorter events, 2.1 us)
Async XLA Ops:
  7.2 95.0 %copy-start = (bf16[2,1024,128]{2,1,0:T(8,128)(2,1)S(1)}, bf16[2,1024,128]{2,1,0:T(8,128)(2,1)}, u32[]{:S(2)}) copy-start(bf16[2,1024,128]{2,1,0:T(8,128)(2,1)} %param.11) | copy-start | bytes 1572868
  7.2 34.2 %copy-start.7 = (bf16[256,1024]{1,0:T(8,128)(2,1)S(1)}, bf16[256,1024]{1,0:T(8,128)(2,1)}, u32[]{:S(2)}) copy-start(bf16[256,1024]{1,0:T(8,128)(2,1)} %param.7) | copy-start | bytes 1572868
  7.2 61.4 %all-gather.3.cloned.1.call-start = ((), (), s32[]{:S(2)}) async-start(), calls=%async_computation.4 | async-start | bytes 3932160 | tf_op jit(solution)/shard_map/all_gather | solution.py:99
  41.4 57.2 %all-gather.5.cloned.1.call-start = ((), (), s32[]{:S(2)}) async-start(), calls=%async_computation.5 | async-start | bytes 3932160 | tf_op jit(solution)/shard_map/all_gather | solution.py:98
  98.6 2.4 %copy-start.5 = (bf16[2,1024,128]{2,1,0:T(8,128)(2,1)S(1)}, bf16[2,1024,128]{2,1,0:T(8,128)(2,1)}, u32[]{:S(2)}) copy-start(bf16[2,1024,128]{2,1,0:T(8,128)(2,1)} %param.12) | copy-start | bytes 1572868
  101.0 2.4 %copy-start.2 = (bf16[2,8,96,1024]{3,2,1,0:T(8,128)(2,1)}, bf16[2,8,96,1024]{3,2,1,0:T(8,128)(2,1)S(1)}, u32[]{:S(2)}) copy-start(bf16[2,8,96,1024]{3,2,1,0:T(8,128)(2,1)S(1)} %copy.106) | copy-start | bytes 9437188
  101.0 3.2 %copy-start.3 = (bf16[2,8,96,1024]{3,2,1,0:T(8,128)(2,1)S(1)}, bf16[2,8,96,1024]{3,2,1,0:T(8,128)(2,1)}, u32[]{:S(2)}) copy-start(bf16[2,8,96,1024]{3,2,1,0:T(8,128)(2,1)} %copy.105) | copy-start | bytes 9437188
  101.0 3.3 %copy-start.12 = (bf16[2,128,1024]{2,1,0:T(8,128)(2,1)S(1)}, bf16[2,128,1024]{2,1,0:T(8,128)(2,1)}, u32[]{:S(2)}) copy-start(bf16[2,128,1024]{2,1,0:T(8,128)(2,1)} %param.13) | copy-start | bytes 1572868
  102.2 3.4 %copy-start.9 = (bf16[2,768,128]{1,2,0:T(8,128)(2,1)}, bf16[2,768,128]{1,2,0:T(8,128)(2,1)S(1)}, u32[]{:S(2)}) copy-start(bf16[2,768,128]{1,2,0:T(8,128)(2,1)S(1)} %convolution_convert_fusion.1) | copy-start | bytes 1179652
  105.6 1.0 copy-start.6
  107.8 3.1 %copy-start.1 = (f32[2,768,1024]{2,1,0:T(8,128)}, f32[2,768,1024]{2,1,0:T(8,128)S(1)}, u32[]{:S(2)}) copy-start(f32[2,768,1024]{2,1,0:T(8,128)S(1)} %convolution_add_fusion) | copy-start | bytes 18874372
  110.8 3.7 %collective-permute-start = (f16[2,768,512]{2,1,0:T(8,128)(2,1)}, f16[2,768,512]{2,1,0:T(8,128)(2,1)S(1)}, u32[]{:S(2)}, u32[]{:S(2)}) collective-permute-start(f16[2,768,512]{2,1,0:T(8,128)(2,1)} %multiply_convert_fusion.1), channel_id=1, source_target_pairs={{0,1},{1,0},{2,3},{3,2},{4,5},{5,4},{6,7},{7,6},{8,9},{9,8},{10,11... | collective-permute-start | bytes 4718600 | tf_op jit(solution)/shard_map/ppermute | solution.py:116
  111.1 3.4 %collective-permute-start.1 = (f32[2,2,768]{2,1,0:T(2,128)S(1)}, f32[2,2,768]{2,1,0:T(2,128)S(1)}, u32[]{:S(2)}, u32[]{:S(2)}) collective-permute-start(f32[2,2,768]{2,1,0:T(2,128)S(1)} %pad_maximum_fusion), channel_id=1, source_target_pairs={{0,1},{1,0},{2,3},{3,2},{4,5},{5,4},{6,7},{7,6},{8,9},{9,8},{10,11... | collective-permute-start | bytes 36872 | tf_op jit(solution)/shard_map/ppermute | solution.py:117
  118.0 12.1 %all-to-all-start.3 = ((f32[8,2,2,96]{3,2,1,0:T(2,128)}), f32[8,2,2,96]{3,2,1,0:T(2,128)S(1)}, u32[]{:S(2)}, u32[]{:S(2)}) async-start(f32[8,2,2,96]{3,2,1,0:T(2,128)} %copy.112), calls=%async_computation.3 | async-start | bytes 32768 | tf_op jit(solution)/shard_map/all_to_all | solution.py:126
  126.0 7.8 %copy-start.11 = (f32[256,2]{0,1:T(2,128)S(1)}, f32[256,2]{0,1:T(2,128)}, u32[]{:S(2)}) copy-start(f32[256,2]{0,1:T(2,128)} %param.10) | copy-start | bytes 6148
  130.1 40.6 %all-to-all-start.2 = ((f16[8,2,96,512]{3,2,1,0:T(8,128)(2,1)}), f16[8,2,96,512]{3,2,1,0:T(8,128)(2,1)S(1)}, u32[]{:S(2)}, u32[]{:S(2)}) async-start(f16[8,2,96,512]{3,2,1,0:T(8,128)(2,1)} %bitcast.55), calls=%async_computation.2 | async-start | bytes 3145728 | tf_op jit(solution)/shard_map/all_to_all | solution.py:125
  134.6 36.0 %copy-start.8 = (pred[256,1536]{1,0:T(8,128)(4,1)}, pred[256,1536]{1,0:T(8,128)(4,1)S(1)}, u32[]{:S(2)}) copy-start(pred[256,1536]{1,0:T(8,128)(4,1)S(1)} %fusion.1) | copy-start | bytes 1179652
  171.5 2.5 %copy-start.4 = (bf16[2,8,96,1024]{3,2,1,0:T(8,128)(2,1)S(1)}, bf16[2,8,96,1024]{3,2,1,0:T(8,128)(2,1)}, u32[]{:S(2)}) copy-start(bf16[2,8,96,1024]{3,2,1,0:T(8,128)(2,1)} %copy.105) | copy-start | bytes 9437188
  171.5 2.5 %copy-start.10 = (bf16[2,768,128]{1,2,0:T(8,128)(2,1)S(1)}, bf16[2,768,128]{1,2,0:T(8,128)(2,1)}, u32[]{:S(2)}) copy-start(bf16[2,768,128]{1,2,0:T(8,128)(2,1)} %copy-done.9) | copy-start | bytes 1179652
  173.4 11.9 %collective-permute-start.2 = (f32[256,512]{1,0:T(8,128)S(1)}, f32[256,512]{1,0:T(8,128)S(1)}, u32[]{:S(2)}, u32[]{:S(2)}) collective-permute-start(f32[256,512]{1,0:T(8,128)S(1)} %fusion.7), channel_id=1, source_target_pairs={{0,2},{1,3},{2,0},{3,1},{4,6},{5,7},{6,4},{7,5},{8,10},{9,11},{10,... | collective-permute-start | bytes 1572872 | tf_op jit(solution)/shard_map/ppermute | solution.py:145
  176.7 13.0 %collective-permute-start.4 = (f32[512]{0:T(512)S(1)}, f32[512]{0:T(512)S(1)}, u32[]{:S(2)}, u32[]{:S(2)}) collective-permute-start(f32[512]{0:T(512)S(1)} %reshape.135), channel_id=1, source_target_pairs={{0,2},{1,3},{2,0},{3,1},{4,6},{5,7},{6,4},{7,5},{8,10},{9,11},{10,... | collective-permute-start | bytes 6152 | tf_op jit(solution)/shard_map/ppermute | solution.py:146
  185.4 5.1 %collective-permute-start.3 = (bf16[256,512]{1,0:T(8,128)(2,1)S(1)}, bf16[256,512]{1,0:T(8,128)(2,1)S(1)}, u32[]{:S(2)}, u32[]{:S(2)}) collective-permute-start(bf16[256,512]{1,0:T(8,128)(2,1)S(1)} %add_convert_fusion), channel_id=1, source_target_pairs={{0,1},{1,0},{2,3},{3,2},{4,5},{5,4},{6,7},{7,6},{8,9},{9,8},{10,11... | collective-permute-start | bytes 786440 | tf_op jit(solution)/shard_map/ppermute | solution.py:148
Sparse Core Ops, SparseCore 0:
  41.5 27.0 all-gather.2
  70.2 28.3 all-gather.4
